TPU v7x, 32 devices: a whole 2x2x4 slice. The times are simulated.
32 devices in a mesh: sp: 4 (over z), tp: 4 (over y, x), dp: 2 (over core).
Axes of the slice: x: 2, y: 2, z: 4, core: 2. Of those that a mesh axis runs over, the one named last changes fastest.
Arguments:
- latent_in: bfloat16 [3072, 2048], P(('dp', 'sp', 'tp')), parts along dimension 0, may hold values from -6 to 6
- condition: bfloat16 [4096], P(('dp', 'sp')), parts along dimension 0, may hold values from -8 to 8
- context_latent: bfloat16 [1024, 256], P(('dp', 'sp')), parts along dimension 0, may hold values from -6 to 6
- context_rope: bfloat16 [1024, 64], P(('dp', 'sp')), parts along dimension 0, may hold values from -6 to 6
- shift_weight: bfloat16 [2048, 2048], P('sp', 'tp'), may hold values from -0.125 to 0.125
- scale_weight: bfloat16 [2048, 2048], P('sp', 'tp'), may hold values from -0.125 to 0.125
- gate_weight: bfloat16 [2048, 2048], P('sp', 'tp'), may hold values from -0.125 to 0.125
- norm_gain: float32 [2048], replicated, may hold values from 0.1 to 1.9
- down_query: bfloat16 [2048, 512], replicated, may hold values from -0.125 to 0.125
- down_latent: bfloat16 [2048, 256], replicated, may hold values from -0.125 to 0.125
- down_rope: bfloat16 [2048, 64], replicated, may hold values from -0.125 to 0.125
- query_gain: float32 [512], replicated, may hold values from 0.5 to 60
- latent_gain: float32 [256], replicated, may hold values from 0.1 to 1.9
- up_query: bfloat16 [512, 1536], P(None, 'tp'), may hold values from -0.25 to 0.25
- up_key: bfloat16 [256, 1024], P(None, 'tp'), may hold values from -0.375 to 0.375
- up_value: bfloat16 [256, 1024], P(None, 'tp'), may hold values from -0.375 to 0.375
- context_bias: float32 [8], P('tp'), may hold values from 1 to 2.5
- out_weight: bfloat16 [1024, 2048], replicated, may hold values from -3 to 3
Outputs:
- mixed_out: bfloat16 [3072, 2048], P(('dp', 'sp', 'tp')), parts along dimension 0
There are 2 independent parts, one for each index of `dp`. A program takes and returns all parts, laid end to end along the dimension named above; an argument that names none is the same for every part. Nothing has to cross between parts.
All inputs are finite; a program needn't handle non-finite values.
Results may differ from a plain program's by a relative error of at most 0.039.
The roundings to bfloat16 on the way count: a program that leaves them out, or rounds other values in their place, can miss the bound.
Values may be sent and summed in bfloat16 or wider, within the bound.
A program may use at most 128 MiB of HBM per device.

v0:
```python
import jax
import jax.numpy as jnp
from jax import lax
from jax.sharding import PartitionSpec as P

QK_NOPE = 128
QK_ROPE = 64
V_HEAD = 128
GRID_W = 64


epsilon = 1e-06
rope_base = 10000.0
block_limit = 2048


def rms_scaled(values, gain_vec):
    mean_sq = jnp.mean(values * values, axis=-1, keepdims=True)
    return values * lax.rsqrt(mean_sq + epsilon) * gain_vec


def rope_tables(positions, rope_width):
    freq_count = rope_width // 4
    inverse = rope_base ** (-jnp.arange(freq_count, dtype=jnp.float32) / freq_count)
    grid_row = (positions // GRID_W).astype(jnp.float32)
    grid_col = (positions % GRID_W).astype(jnp.float32)
    row_angle = grid_row[:, None] * inverse
    col_angle = grid_col[:, None] * inverse
    angles = jnp.concatenate([row_angle, row_angle, col_angle, col_angle], axis=-1)
    return (jnp.cos(angles), jnp.sin(angles))


def rope_turn(values, cosine_table, sine_table):
    part_one, part_two, part_three, part_four = jnp.split(values, 4, axis=-1)
    turned = jnp.concatenate([-part_two, part_one, -part_four, part_three], axis=-1)
    return values * cosine_table + turned * sine_table


def attend(attn_state, query_nope, query_rope, keys_nope, values_in, keys_rope, bias_col):
    score_scale = (query_nope.shape[-1] + query_rope.shape[-1]) ** (-0.5)
    scores = jnp.einsum("thd,khd->htk", query_nope, keys_nope, preferred_element_type=jnp.float32)
    scores = scores + jnp.einsum(
        "thr,kr->htk", query_rope, keys_rope, preferred_element_type=jnp.float32
    )
    scores = scores * score_scale + bias_col
    run_max, run_total, run_acc = attn_state
    new_max = jnp.maximum(run_max, jnp.max(scores, axis=-1))
    shrink = jnp.exp(run_max - new_max)
    weights = jnp.exp(scores - new_max[:, :, None])
    new_total = run_total * shrink + jnp.sum(weights, axis=-1)
    new_acc = run_acc * shrink[:, :, None] + jnp.einsum(
        "htk,khd->htd", weights.astype(jnp.bfloat16), values_in, preferred_element_type=jnp.float32
    )
    return (new_max, new_total, new_acc)


def over_blocks(attn_state, arrays, handle):
    row_count = arrays[0].shape[0]
    block_rows = 1
    for candidate in range(min(row_count, block_limit), 0, -1):
        if row_count % candidate == 0:
            block_rows = candidate
            break
    block_count = row_count // block_rows
    if block_count == 1:
        return handle(attn_state, arrays)
    stacked = tuple(
        (array_in.reshape((block_count, block_rows) + array_in.shape[1:]) for array_in in arrays)
    )

    def one_turn(inner_state, pieces):
        return (handle(inner_state, pieces), None)

    return lax.scan(one_turn, attn_state, stacked)[0]


def on_device(
    latent_in,
    condition,
    context_latent,
    context_rope,
    shift_weight,
    scale_weight,
    gate_weight,
    norm_gain,
    down_query,
    down_latent,
    down_rope,
    query_gain,
    latent_gain,
    up_query,
    up_key,
    up_value,
    context_bias,
    out_weight,
):
    activated = jax.nn.silu(condition.astype(jnp.float32)).astype(jnp.bfloat16)
    partials = jnp.stack(
        [
            jnp.dot(activated, weight_in, preferred_element_type=jnp.float32)
            for weight_in in (shift_weight, scale_weight, gate_weight)
        ]
    )
    summed = lax.psum(partials, "sp")
    modulation = lax.all_gather(summed, "tp", axis=1, tiled=True)
    shift_vec = modulation[0]
    scale_vec = modulation[1]
    gate_vec = modulation[2]
    residual_in = latent_in.astype(jnp.float32)
    normed = (rms_scaled(residual_in, norm_gain) * (1.0 + scale_vec) + shift_vec).astype(
        jnp.bfloat16
    )
    query_low = rms_scaled(
        jnp.dot(normed, down_query, preferred_element_type=jnp.float32), query_gain
    ).astype(jnp.bfloat16)
    latent_low = rms_scaled(
        jnp.dot(normed, down_latent, preferred_element_type=jnp.float32), latent_gain
    ).astype(jnp.bfloat16)
    local_rows = latent_in.shape[0]
    first_row = (lax.axis_index("sp") * lax.axis_size("tp") + lax.axis_index("tp")) * local_rows
    own_positions = first_row + jnp.arange(local_rows, dtype=jnp.int32)
    own_cosine, own_sine = rope_tables(own_positions, QK_ROPE)
    rope_keys = rope_turn(
        jnp.dot(normed, down_rope, preferred_element_type=jnp.float32), own_cosine, own_sine
    ).astype(jnp.bfloat16)
    query_group, latent_group, rope_group = (
        lax.all_gather(query_low, "tp", axis=0, tiled=True),
        lax.all_gather(latent_low, "tp", axis=0, tiled=True),
        lax.all_gather(rope_keys, "tp", axis=0, tiled=True),
    )
    group_rows = query_group.shape[0]
    group_positions = lax.axis_index("sp") * group_rows + jnp.arange(group_rows, dtype=jnp.int32)
    group_cosine, group_sine = rope_tables(group_positions, QK_ROPE)
    head_count = up_key.shape[1] // QK_NOPE
    queries = jnp.dot(query_group, up_query, preferred_element_type=jnp.float32).reshape(
        group_rows, head_count, QK_NOPE + QK_ROPE
    )
    query_nope = queries[:, :, :QK_NOPE].astype(jnp.bfloat16)
    query_rope = rope_turn(
        queries[:, :, QK_NOPE:], group_cosine[:, None, :], group_sine[:, None, :]
    ).astype(jnp.bfloat16)
    context_all, context_keys_rope = (
        lax.all_gather(context_latent, "sp", axis=0, tiled=True),
        lax.all_gather(context_rope, "sp", axis=0, tiled=True),
    )
    context_count = context_all.shape[0]
    context_nope = (
        jnp.dot(context_all, up_key, preferred_element_type=jnp.float32)
        .astype(jnp.bfloat16)
        .reshape(context_count, head_count, QK_NOPE)
    )
    context_values = (
        jnp.dot(context_all, up_value, preferred_element_type=jnp.float32)
        .astype(jnp.bfloat16)
        .reshape(context_count, head_count, V_HEAD)
    )
    start_state = (
        jnp.full((head_count, group_rows), -jnp.inf, jnp.float32),
        jnp.zeros((head_count, group_rows), jnp.float32),
        jnp.zeros((head_count, group_rows, V_HEAD), jnp.float32),
    )
    bias_col = context_bias[:, None, None]

    def context_step(inner_state, pieces):
        return attend(
            inner_state, query_nope, query_rope, pieces[0], pieces[1], pieces[2], bias_col
        )

    attn_state = over_blocks(
        start_state, (context_nope, context_values, context_keys_rope), context_step
    )
    own_nope = jnp.dot(latent_group, up_key, preferred_element_type=jnp.float32).astype(
        jnp.bfloat16
    )
    own_values = jnp.dot(latent_group, up_value, preferred_element_type=jnp.float32).astype(
        jnp.bfloat16
    )

    def expanded_step(inner_state, pieces):
        piece_rows = pieces[0].shape[0]
        return attend(
            inner_state,
            query_nope,
            query_rope,
            pieces[0].reshape(piece_rows, head_count, QK_NOPE),
            pieces[1].reshape(piece_rows, head_count, V_HEAD),
            pieces[2],
            0.0,
        )

    attn_state = over_blocks(
        attn_state,
        (
            lax.all_gather(own_nope, "sp", axis=0, tiled=True),
            lax.all_gather(own_values, "sp", axis=0, tiled=True),
            lax.all_gather(rope_group, "sp", axis=0, tiled=True),
        ),
        expanded_step,
    )
    attended = (attn_state[2] / attn_state[1][:, :, None]).astype(jnp.bfloat16)
    attended = attended.transpose(1, 0, 2).reshape(group_rows, head_count * V_HEAD)
    token_major = lax.all_to_all(attended, "tp", split_axis=0, concat_axis=1, tiled=True)
    mixed = jnp.dot(token_major, out_weight, preferred_element_type=jnp.float32)
    return (residual_in + gate_vec * mixed).astype(jnp.bfloat16)


def solution(mesh):
    in_specs = (
        P(("dp", "sp", "tp"), None),
        P(("dp", "sp")),
        P(("dp", "sp"), None),
        P(("dp", "sp"), None),
        P("sp", "tp"),
        P("sp", "tp"),
        P("sp", "tp"),
        P(),
        P(),
        P(),
        P(),
        P(),
        P(),
        P(None, "tp"),
        P(None, "tp"),
        P(None, "tp"),
        P("tp"),
        P(),
    )
    out_specs = P(("dp", "sp", "tp"), None)
    return jax.shard_map(
        on_device, mesh=mesh, in_specs=in_specs, out_specs=out_specs, check_vma=False
    )
```

profile of v0, /device:TPU:0, one launch (start us, length us, event | category | flops | bytes accessed | tf_op | source)
XLA Modules:
  0.0 158.6 jit_solution(2897633564219635338)
XLA Ops:
  1.3 1.2 fusion.72
  2.6 1.2 fusion.73
  3.8 1.3 fusion.74
  5.1 13.8 %psum.7 = f32[3,512]{1,0:T(4,128)S(1)} all-reduce(f32[3,512]{1,0:T(4,128)S(1)} %pad_maximum_fusion.2), channel_id=1, replica_groups=mesh['sp'=4,'tp'=4,'dp'=2] {'sp'}, use_global_device_ids=true, to_apply=%region_0.1 | all-reduce | flops 1536 | bytes 12288 | tf_op jit(solution)/shard_map/psum | solution.py:104
  18.9 8.2 %all_gather.27 = f32[3,2048]{1,0:T(4,128)S(1)} all-gather(f32[3,512]{1,0:T(4,128)S(1)} %psum.7), channel_id=1, replica_groups=mesh['sp'=4,'tp'=4,'dp'=2] {'tp'}, dimensions={1}, use_global_device_ids=true | all-gather | bytes 30720 | tf_op jit(solution)/shard_map/all_gather | solution.py:105
  27.1 1.2 fusion.26
  28.4 1.9 %multiply_reduce_fusion.1 = (f32[96]{0:T(128)S(1)}, f32[96,256]{1,0:T(8,128)S(1)}) fusion(bf16[2048,256]{1,0:T(8,128)(2,1)} %param.27, bf16[96,2048]{1,0:T(8,128)(2,1)} %param.18, f32[2048]{0:T(1024)S(1)} %bitcast.119, f32[2048]{0:T(1024)S(1)} %bitcast.122, f32[2048]{0:T(1024)} %param.25, f32[96]{0:T(128)S(1)} %add_rsqrt_fusion.2), kind=kOutput, calls=%fused_computation.50 | convolution fusion | flops 101892000 | bytes 1565440 | tf_op jit(solution)/shard_map/dot_general | solution.py:117
  30.3 8.7 %all_gather.31 = bf16[384,256]{1,0:T(8,128)(2,1)S(1)} all-gather(bf16[96,256]{1,0:T(8,128)(2,1)S(1)} %multiply_convert_fusion.1), channel_id=1, replica_groups=mesh['sp'=4,'tp'=4,'dp'=2] {'tp'}, dimensions={0}, use_global_device_ids=true | all-gather | bytes 245760 | tf_op jit(solution)/shard_map/all_gather | solution.py:128
  39.1 13.8 %all_gather.29 = bf16[512,256]{1,0:T(8,128)(2,1)S(1)} all-gather(bf16[128,256]{1,0:T(8,128)(2,1)S(1)} %copy-done.12), channel_id=1, replica_groups=mesh['sp'=4,'tp'=4,'dp'=2] {'sp'}, dimensions={0}, use_global_device_ids=true | all-gather | bytes 327680 | tf_op jit(solution)/shard_map/all_gather | solution.py:143
  52.9 0.9 convolution_convert_fusion.3
  54.0 1.0 convolution_convert_fusion
  56.0 8.5 %all_gather.28 = bf16[384,512]{1,0:T(8,128)(2,1)S(1)} all-gather(bf16[96,512]{1,0:T(8,128)(2,1)S(1)} %multiply_convert_fusion), channel_id=1, replica_groups=mesh['sp'=4,'tp'=4,'dp'=2] {'tp'}, dimensions={0}, use_global_device_ids=true | all-gather | bytes 491520 | tf_op jit(solution)/shard_map/all_gather | solution.py:127
  66.3 1.3 fusion.62
  69.6 0.9 fusion.47
  70.5 8.2 %all-gather = bf16[4,96,64]{1,2,0:T(8,128)(2,1)S(1)} all-gather(bf16[1,96,64]{1,2,0:T(8,128)(2,1)S(1)} %fusion.47), channel_id=1, replica_groups=mesh['sp'=4,'tp'=4,'dp'=2] {'tp'}, dimensions={0}, use_global_device_ids=true | all-gather | bytes 61440 | tf_op jit(solution)/shard_map/all_gather | solution.py:129
  79.4 1.6 reshape.254
  81.0 14.6 %all_gather.34 = bf16[1536,64]{0,1:T(8,128)(2,1)S(1)} all-gather(bf16[384,64]{0,1:T(8,128)(2,1)} %reshape.254), channel_id=1, replica_groups=mesh['sp'=4,'tp'=4,'dp'=2] {'sp'}, dimensions={0}, use_global_device_ids=true | all-gather | bytes 245760 | tf_op jit(solution)/shard_map/all_gather | solution.py:196
  95.6 16.9 %all_gather.32 = bf16[1536,256]{1,0:T(8,128)(2,1)S(1)} all-gather(bf16[384,256]{1,0:T(8,128)(2,1)} %convolution_convert_fusion.3), channel_id=1, replica_groups=mesh['sp'=4,'tp'=4,'dp'=2] {'sp'}, dimensions={0}, use_global_device_ids=true | all-gather | bytes 983040 | tf_op jit(solution)/shard_map/all_gather | solution.py:194
  112.9 12.2 %all_gather.30 = bf16[512,64]{0,1:T(8,128)(2,1)S(1)} all-gather(bf16[128,64]{0,1:T(8,128)(2,1)S(1)} %copy-done.13), channel_id=1, replica_groups=mesh['sp'=4,'tp'=4,'dp'=2] {'sp'}, dimensions={0}, use_global_device_ids=true | all-gather | bytes 81920 | tf_op jit(solution)/shard_map/all_gather | solution.py:144
  126.3 1.0 fusion.71
  128.3 15.6 %all_gather.35 = bf16[1536,256]{1,0:T(8,128)(2,1)S(1)} all-gather(bf16[384,256]{1,0:T(8,128)(2,1)S(1)} %convolution_convert_fusion.2), channel_id=1, replica_groups=mesh['sp'=4,'tp'=4,'dp'=2] {'sp'}, dimensions={0}, use_global_device_ids=true | all-gather | bytes 983040 | tf_op jit(solution)/shard_map/all_gather | solution.py:195
  145.5 0.9 fusion.23
  146.8 8.1 %all_to_all.19 = bf16[4,96,256]{2,1,0:T(8,128)(2,1)S(1)} all-to-all(bf16[4,96,256]{2,1,0:T(8,128)(2,1)S(1)} %all_to_all.14), channel_id=1, replica_groups=mesh['sp'=4,'tp'=4,'dp'=2] {'tp'}, dimensions={0} | all-to-all | bytes 393216 | tf_op jit(solution)/shard_map/all_to_all | solution.py:202
  154.9 3.8 %fusion.7 = bf16[96,2048]{1,0:T(8,128)(2,1)} fusion(bf16[96,1024]{1,0:T(8,128)(2,1)S(1)} %bitcast.116, bf16[1024,2048]{1,0:T(8,128)(2,1)} %param.35, bf16[96,2048]{1,0:T(8,128)(2,1)S(1)} %copy-done.1, f32[2048]{0:T(1024)S(1)} %bitcast.118), kind=kOutput, calls=%fused_computation.9 | convolution fusion | flops 403439616 | bytes 5185536 | tf_op jit(solution)/shard_map/dot_general | solution.py:203
  (80 shorter events, 11.5 us)
Async XLA Ops:
  0.0 55.3 %copy-start = (bf16[2048,512]{1,0:T(8,128)(2,1)S(1)}, bf16[2048,512]{1,0:T(8,128)(2,1)}, u32[]{:S(2)}) copy-start(bf16[2048,512]{1,0:T(8,128)(2,1)} %param.26) | copy-start | bytes 6291460
  0.0 30.2 %copy-start.19 = (f32[256]{0:T(256)S(1)}, f32[256]{0:T(256)}, u32[]{:S(2)}) copy-start(f32[256]{0:T(256)} %param.30) | copy-start | bytes 3076
  0.0 39.0 %copy-start.12 = (bf16[128,256]{1,0:T(8,128)(2,1)S(1)}, bf16[128,256]{1,0:T(8,128)(2,1)}, u32[]{:S(2)}) copy-start(bf16[128,256]{1,0:T(8,128)(2,1)} %param.20) | copy-start | bytes 196612
  1.3 51.5 %copy-start.3 = (bf16[256,256]{1,0:T(8,128)(2,1)S(1)}, bf16[256,256]{1,0:T(8,128)(2,1)}, u32[]{:S(2)}) copy-start(bf16[256,256]{1,0:T(8,128)(2,1)} %param.32) | copy-start | bytes 393220
  3.8 50.2 %copy-start.4 = (bf16[256,256]{1,0:T(8,128)(2,1)S(1)}, bf16[256,256]{1,0:T(8,128)(2,1)}, u32[]{:S(2)}) copy-start(bf16[256,256]{1,0:T(8,128)(2,1)} %param.33) | copy-start | bytes 393220
  27.1 28.1 %copy-start.14 = (f32[1,2048]{1,0:T(1,128)}, f32[1,2048]{1,0:T(1,128)S(1)}, u32[]{:S(2)}) copy-start(f32[1,2048]{1,0:T(1,128)S(1)} %get-tuple-element.15) | copy-start | bytes 24580
  27.1 27.9 %copy-start.5 = (bf16[256,256]{1,0:T(8,128)(2,1)S(1)}, bf16[256,256]{1,0:T(8,128)(2,1)}, u32[]{:S(2)}) copy-start(bf16[256,256]{1,0:T(8,128)(2,1)} %param.33) | copy-start | bytes 393220
  28.3 26.9 %copy-start.22 = (f32[96]{0:T(128)}, f32[96]{0:T(128)S(1)}, u32[]{:S(2)}) copy-start(f32[96]{0:T(128)S(1)} %add_rsqrt_fusion.2) | copy-start | bytes 1156
  28.3 26.9 %copy-start.1 = (bf16[96,2048]{1,0:T(8,128)(2,1)S(1)}, bf16[96,2048]{1,0:T(8,128)(2,1)}, u32[]{:S(2)}) copy-start(bf16[96,2048]{1,0:T(8,128)(2,1)} %param.18) | copy-start | bytes 1179652
  28.4 26.9 %copy-start.21 = (f32[2048]{0:T(1024)S(1)}, f32[2048]{0:T(1024)}, u32[]{:S(2)}) copy-start(f32[2048]{0:T(1024)} %param.25) | copy-start | bytes 24580
  53.7 2.2 %copy-start.17 = (f32[512]{0:T(512)S(1)}, f32[512]{0:T(512)}, u32[]{:S(2)}) copy-start(f32[512]{0:T(512)} %param.29) | copy-start | bytes 6148
  54.0 10.5 %copy-start.6 = (bf16[512,384]{1,0:T(8,128)(2,1)S(1)}, bf16[512,384]{1,0:T(8,128)(2,1)}, u32[]{:S(2)}) copy-start(bf16[512,384]{1,0:T(8,128)(2,1)} %param.31) | copy-start | bytes 1179652
  67.6 0.6 copy-start.11
  70.5 54.6 %copy-start.15 = (f32[384]{0:T(512)S(1)}, f32[384]{0:T(512)}, u32[]{:S(2)}) copy-start(f32[384]{0:T(512)} %get-tuple-element.33) | copy-start | bytes 4612
  70.5 54.6 %copy-start.16 = (f32[384]{0:T(512)S(1)}, f32[384]{0:T(512)}, u32[]{:S(2)}) copy-start(f32[384]{0:T(512)} %get-tuple-element.34) | copy-start | bytes 4612
  81.0 31.9 %copy-start.13 = (bf16[128,64]{0,1:T(8,128)(2,1)S(1)}, bf16[128,64]{0,1:T(8,128)(2,1)}, u32[]{:S(2)}) copy-start(bf16[128,64]{0,1:T(8,128)(2,1)} %param.21) | copy-start | bytes 49156
  81.0 44.1 %copy-start.18 = (f32[16]{0:T(128)S(1)}, f32[16]{0:T(128)}, u32[]{:S(2)}) copy-start(f32[16]{0:T(128)} %multiply_power_fusion) | copy-start | bytes 196
  81.0 44.4 %copy-start.7 = (f32[384,2,16]{0,2,1:T(8,128)S(1)}, f32[384,2,16]{0,2,1:T(8,128)}, u32[]{:S(2)}) copy-start(f32[384,2,16]{0,2,1:T(8,128)} %get-tuple-element.7) | copy-start | bytes 147460
  81.0 44.4 %copy-start.8 = (f32[384,2,16]{0,2,1:T(8,128)S(1)}, f32[384,2,16]{0,2,1:T(8,128)}, u32[]{:S(2)}) copy-start(f32[384,2,16]{0,2,1:T(8,128)} %get-tuple-element.8) | copy-start | bytes 147460
  81.0 44.4 %copy-start.9 = (f32[384,2,16]{0,2,1:T(8,128)S(1)}, f32[384,2,16]{0,2,1:T(8,128)}, u32[]{:S(2)}) copy-start(f32[384,2,16]{0,2,1:T(8,128)} %get-tuple-element.9) | copy-start | bytes 147460
  81.0 44.4 %copy-start.10 = (f32[384,2,16]{0,2,1:T(8,128)S(1)}, f32[384,2,16]{0,2,1:T(8,128)}, u32[]{:S(2)}) copy-start(f32[384,2,16]{0,2,1:T(8,128)} %get-tuple-element.10) | copy-start | bytes 147460
  126.3 1.0 copy-start.20
  143.8 1.0 copy-start.2
where the time goes:
time: 159 us
  blocking collectives  129 us (81%)
  matrix products  18.4 us (12%)
  other arithmetic  7.9 us (5%)
  local copies, waits for them, and re-layouts  3.43 us (2%)
    all_gather x1, blocking collectives, on_device(): lax.all_gather(own_nope, 'sp', axis=0, tiled=True)  16.9 us
    all_gather x1, blocking collectives, on_device(): lax.all_gather(own_values, 'sp', axis=0, tiled=True)  15.6 us
    all_gather x1, blocking collectives, on_device(): lax.all_gather(rope_group, 'sp', axis=0, tiled=True)  14.6 us
    all_gather x1, blocking collectives, on_device(): lax.all_gather(context_latent, 'sp', axis=0, tiled=True)  13.8 us
    psum x1, blocking collectives, on_device(): summed = lax.psum(partials, 'sp')  13.8 us
    all_gather x1, blocking collectives, on_device(): lax.all_gather(context_rope, 'sp', axis=0, tiled=True)  12.2 us
    all_gather x1, blocking collectives, on_device(): lax.all_gather(latent_low, 'tp', axis=0, tiled=True)  8.7 us
    all_gather x1, blocking collectives, on_device(): lax.all_gather(query_low, 'tp', axis=0, tiled=True)  8.53 us

commit v1 on v0

v1 whole, which is shorter than its diff:
```python
import functools
import math

import jax
import jax.numpy as jnp
from jax import lax
from jax.experimental import pallas as pl
from jax.experimental.pallas import tpu as pltpu
from jax.sharding import PartitionSpec as P

QK_NOPE = 128
QK_ROPE = 64
V_HEAD = 128
GRID_W = 64
EPS = 1e-06
ROPE_BASE = 10000.0
F32 = jnp.float32
BF16 = jnp.bfloat16
LOG2E = 1.4426950408889634


def dot(a, b):
    return jnp.dot(a, b, preferred_element_type=F32)


def dot_t(a, b):
    return lax.dot_general(a, b, (((1,), (1,)), ((), ())), preferred_element_type=F32)


def rms(values, gain):
    mean_sq = jnp.mean(values * values, axis=-1, keepdims=True)
    return values * lax.rsqrt(mean_sq + EPS) * gain


def turn(u, cos, sin_up, sin_down):
    width = u.shape[1]
    return u * cos + pltpu.roll(u, width - 16, 1) * sin_up + pltpu.roll(u, 16, 1) * sin_down


def kernel(sp, tp, *refs):
    (
        latent_hbm, cond_ref, ctx_lat_hbm, ctx_rope_hbm, shift_hbm, scale_hbm, gate_hbm,
        norm_gain_ref, dq_hbm, dl_hbm, dr_hbm, q_gain_ref, l_gain_ref, uq_hbm, uk_hbm, uv_hbm,
        bias_ref, ow_hbm, inv_ref,
        out_ref,
        x_ref, shift_w, scale_w, gate_w, dq, dl, dr, uq, uk, uv, ow, ctx_rope,
        base, cos_tab, sup_tab, sdn_tab, mod_z, mod_t, ctx_buf, lat_buf, q_buf, att_src, att_buf,
        mix, load_sem,
        mz_send, mz_recv, mt_send, mt_recv, cx_send, cx_recv, lz_send, lt_send, l_recv,
        q_send, q_recv, a_send, a_recv,
    ) = refs
    me_s = lax.axis_index("sp")
    me_t = lax.axis_index("tp")
    rows = x_ref.shape[0]
    group = rows * tp
    mcol = shift_w.shape[1]
    kv_rank = uk.shape[0]

    def zpeer(d):
        return lax.rem(me_s + d, sp)

    def tpeer(d):
        return lax.rem(me_t + d, tp)

    def remote(src, dst, ssem, rsem, axis, peer):
        return pltpu.make_async_remote_copy(
            src_ref=src, dst_ref=dst, send_sem=ssem, recv_sem=rsem,
            device_id={axis: peer}, device_id_type=pl.DeviceIdType.MESH,
        )

    loads = {}
    for i, (name, src, dst) in enumerate((
        ("shift", shift_hbm, shift_w), ("scale", scale_hbm, scale_w), ("gate", gate_hbm, gate_w),
        ("cl", ctx_lat_hbm, ctx_buf.at[me_s, :, pl.ds(0, kv_rank)]), ("cr", ctx_rope_hbm, ctx_rope),
        ("x", latent_hbm, x_ref), ("dl", dl_hbm, dl), ("dr", dr_hbm, dr), ("dq", dq_hbm, dq),
        ("uk", uk_hbm, uk), ("uv", uv_hbm, uv), ("uq", uq_hbm, uq), ("ow", ow_hbm, ow),
    )):
        loads[name] = pltpu.make_async_copy(src, dst, load_sem.at[i])
        loads[name].start()

    barrier = pltpu.get_barrier_semaphore()
    for d in range(1, sp):
        pl.semaphore_signal(barrier, inc=1, device_id={"sp": zpeer(d)}, device_id_type=pl.DeviceIdType.MESH)
    for d in range(1, tp):
        pl.semaphore_signal(barrier, inc=1, device_id={"tp": tpeer(d)}, device_id_type=pl.DeviceIdType.MESH)

    sends = []

    cond = cond_ref[...].astype(F32)
    act = (cond / (1.0 + jnp.exp(-cond))).astype(BF16)
    act = jnp.broadcast_to(act, (16, act.shape[1]))
    for i, (name, w) in enumerate((("shift", shift_w), ("scale", scale_w), ("gate", gate_w))):
        loads[name].wait()
        mod_z[me_s, i:i + 1, :] = dot(act, w[...])[0:1]
    mod_z[me_s, 3:4, :] = jnp.zeros((1, mcol), F32)
    pl.semaphore_wait(barrier, sp + tp - 2)
    for d in range(1, sp):
        c = remote(mod_z.at[me_s], mod_z.at[me_s], mz_send.at[d], mz_recv.at[me_s], "sp", zpeer(d))
        c.start()
        sends.append(c)
    loads["cl"].wait()
    loads["cr"].wait()
    cr = ctx_rope[...]
    ctx_buf[me_s, :, kv_rank:] = jnp.concatenate([cr, cr], axis=1)
    for d in range(1, sp):
        c = remote(ctx_buf.at[me_s], ctx_buf.at[me_s], cx_send.at[d], cx_recv.at[me_s], "sp", zpeer(d))
        c.start()
        sends.append(c)
    loads["x"].wait()
    base[...] = rms(x_ref[...].astype(F32), norm_gain_ref[...])

    for d in range(1, sp):
        s = zpeer(d)
        remote(mod_z.at[s], mod_z.at[s], mz_send.at[d], mz_recv.at[s], "sp", s).wait_recv()
    total = mod_z[0]
    for s in range(1, sp):
        total = total + mod_z[s]
    mod_t[me_t] = total
    for d in range(1, tp):
        c = remote(mod_t.at[me_t], mod_t.at[me_t], mt_send.at[d], mt_recv.at[me_t], "tp", tpeer(d))
        c.start()
        sends.append(c)

    pos = me_s * group + lax.broadcasted_iota(jnp.int32, (group, 128), 0)
    lane = lax.broadcasted_iota(jnp.int32, (group, 128), 1)
    coord = jnp.where(lax.rem(lane, 64) < 32, lax.div(pos, GRID_W), lax.rem(pos, GRID_W))
    angle = coord.astype(F32) * inv_ref[...]
    sin = jnp.sin(angle)
    first_run = lax.rem(lane, 32) < 16
    cos_tab[...] = jnp.cos(angle)
    sup_tab[...] = jnp.where(first_run, -sin, 0.0)
    sdn_tab[...] = jnp.where(first_run, 0.0, sin)

    loads["dl"].wait()
    loads["dr"].wait()
    normed = []
    low_l = low_r = None
    for d in range(tp):
        t = tpeer(d)
        if d:
            remote(mod_t.at[t], mod_t.at[t], mt_send.at[d], mt_recv.at[t], "tp", t).wait_recv()
        cols = pl.ds(pl.multiple_of(t * mcol, mcol), mcol)
        m = mod_t[t]
        nd = (base[:, cols] * (1.0 + m[1:2]) + m[0:1]).astype(BF16)
        normed.append((nd, cols))
        pl_, pr_ = dot(nd, dl[cols, :]), dot(nd, dr[cols, :])
        low_l = pl_ if low_l is None else low_l + pl_
        low_r = pr_ if low_r is None else low_r + pr_
    own = pl.ds(pl.multiple_of(me_t * rows, rows), rows)
    lat_buf[me_t, me_s, :, :kv_rank] = rms(low_l, l_gain_ref[...]).astype(BF16)
    lat_buf[me_t, me_s, :, kv_rank:] = turn(
        jnp.concatenate([low_r, low_r], axis=1), cos_tab[own, :], sup_tab[own, :], sdn_tab[own, :]
    ).astype(BF16)
    mine = lat_buf.at[me_t, me_s]
    for d in range(1, sp):
        c = remote(mine, mine, lz_send.at[d], l_recv.at[me_t, me_s], "sp", zpeer(d))
        c.start()
        sends.append(c)
    loads["dq"].wait()
    low_q = None
    for nd, cols in normed:
        pq = dot(nd, dq[cols, :])
        low_q = pq if low_q is None else low_q + pq
    q_buf[me_t] = rms(low_q, q_gain_ref[...]).astype(BF16)
    for d in range(1, tp):
        c = remote(q_buf.at[me_t], q_buf.at[me_t], q_send.at[d], q_recv.at[me_t], "tp", tpeer(d))
        c.start()
        sends.append(c)
    for d in range(1, tp):
        c = remote(mine, mine, lt_send.at[0, d], l_recv.at[me_t, me_s], "tp", tpeer(d))
        c.start()
        sends.append(c)

    def expand(block):
        low = block[:, :kv_rank]
        kn = dot(low, uk[...]).astype(BF16)
        v = dot(low, uv[...]).astype(BF16)
        kr = block[:, kv_rank:]
        return (
            jnp.concatenate([kn[:, :QK_NOPE], kr], axis=1),
            jnp.concatenate([kn[:, QK_NOPE:], kr], axis=1),
            v,
        )

    loads["uk"].wait()
    loads["uv"].wait()
    for d in range(1, sp):
        s = zpeer(d)
        remote(ctx_buf.at[s], ctx_buf.at[s], cx_send.at[d], cx_recv.at[s], "sp", s).wait_recv()
    ctx_kv = expand(ctx_buf[...].reshape(-1, ctx_buf.shape[2]))

    for d in range(1, sp):
        s = zpeer(d)
        slot = lat_buf.at[me_t, s]
        remote(slot, slot, lz_send.at[d], l_recv.at[me_t, s], "sp", s).wait_recv()
        for e in range(1, tp):
            c = remote(slot, slot, lt_send.at[d, e], l_recv.at[me_t, s], "tp", tpeer(e))
            c.start()
            sends.append(c)

    loads["uq"].wait()
    for d in range(1, tp):
        t = tpeer(d)
        remote(q_buf.at[t], q_buf.at[t], q_send.at[d], q_recv.at[t], "tp", t).wait_recv()
    q = dot(q_buf[...].reshape(group, q_buf.shape[2]), uq[...])
    one, two = q[:, 128:256], q[:, 256:384]
    low_half = lax.broadcasted_iota(jnp.int32, (group, 128), 1) < 64
    rope = turn(jnp.where(low_half, one, two), cos_tab[...], sup_tab[...], sdn_tab[...])
    nope = (q[:, :128], pltpu.roll(jnp.where(low_half, two, one), 64, 1))
    heads = (
        jnp.concatenate([nope[0], jnp.where(low_half, rope, 0.0)], axis=1).astype(BF16),
        jnp.concatenate([nope[1], jnp.where(low_half, 0.0, rope)], axis=1).astype(BF16),
    )
    factor = (QK_NOPE + QK_ROPE) ** (-0.5) * LOG2E

    def attend(state, kv, bias):
        result = []
        for h in range(2):
            s = dot_t(heads[h], kv[h]) * factor
            if bias:
                s = s + bias_ref[h] * LOG2E
            top = jnp.max(s, axis=-1, keepdims=True)
            v = kv[2][:, h * V_HEAD:(h + 1) * V_HEAD]
            if state is None:
                p = jnp.exp2(s - top)
                result.append((top, jnp.sum(p, axis=-1, keepdims=True), dot(p.astype(BF16), v)))
            else:
                m0, l0, a0 = state[h]
                top = jnp.maximum(top, m0)
                p = jnp.exp2(s - top)
                shrink = jnp.exp2(m0 - top)
                result.append((
                    top,
                    l0 * shrink + jnp.sum(p, axis=-1, keepdims=True),
                    a0 * shrink + dot(p.astype(BF16), v),
                ))
        return tuple(result)

    state = attend(None, ctx_kv, True)
    span = math.gcd(sp, 4)
    for d in range(tp):
        t = tpeer(d)
        if d:
            for e in range(sp):
                s = zpeer(e)
                slot = lat_buf.at[t, s]
                remote(slot, slot, lt_send.at[e, d], l_recv.at[t, s], "tp", t).wait_recv()

        def chunk(i, st, t=t):
            block = lat_buf[t, pl.ds(i * span, span)]
            return attend(st, expand(block.reshape(span * rows, block.shape[2])), False)

        if sp == span:
            state = chunk(0, state)
        else:
            state = lax.fori_loop(0, sp // span, chunk, state)
    for h in range(2):
        att = (state[h][2] / state[h][1]).astype(BF16)
        att_src[:, :, h * V_HEAD:(h + 1) * V_HEAD] = att.reshape(tp, rows, V_HEAD)
    for d in range(1, tp):
        t = tpeer(d)
        c = remote(att_src.at[t], att_buf.at[me_t], a_send.at[d], a_recv.at[me_t], "tp", t)
        c.start()
        sends.append(c)
    loads["ow"].wait()
    width = att_src.shape[2]
    for d in range(tp):
        t = tpeer(d)
        if d == 0:
            block = att_src[me_t]
        else:
            remote(att_buf.at[t], att_buf.at[t], a_send.at[d], a_recv.at[t], "tp", t).wait_recv()
            block = att_buf[t]
        part = dot(block, ow[pl.ds(pl.multiple_of(t * width, width), width), :])
        if d == 0:
            mix[...] = part
        else:
            mix[...] += part
    for t in range(tp):
        cols = slice(t * mcol, (t + 1) * mcol)
        out_ref[:, cols] = (x_ref[:, cols].astype(F32) + mod_t[t][2:3] * mix[:, cols]).astype(BF16)
    for c in sends:
        c.wait_send()


def solution(mesh):
    sp, tp = mesh.shape["sp"], mesh.shape["tp"]

    def on_device(
        latent_in, condition, context_latent, context_rope, shift_weight, scale_weight,
        gate_weight, norm_gain, down_query, down_latent, down_rope, query_gain, latent_gain,
        up_query, up_key, up_value, context_bias, out_weight,
    ):
        rows, width = latent_in.shape
        n = QK_ROPE // 4
        inverse = ROPE_BASE ** (-jnp.arange(n, dtype=F32) / n)
        inverse = jnp.tile(inverse, 128 // n)[None]
        group = rows * tp
        any_ = pl.BlockSpec(memory_space=pl.ANY)
        vmem = pl.BlockSpec(memory_space=pltpu.VMEM)
        smem = pl.BlockSpec(memory_space=pltpu.SMEM)
        kv_rank, q_rank = down_latent.shape[1], down_query.shape[1]
        heads = up_key.shape[1] // QK_NOPE
        block = kv_rank + 2 * QK_ROPE
        dma = pltpu.SemaphoreType.DMA

        def like(a):
            return pltpu.VMEM(a.shape, a.dtype)

        return pl.pallas_call(
            functools.partial(kernel, sp, tp),
            out_shape=jax.ShapeDtypeStruct(latent_in.shape, latent_in.dtype),
            in_specs=[any_, vmem, any_, any_, any_, any_, any_, vmem, any_, any_, any_, vmem, vmem,
                      any_, any_, any_, smem, any_, vmem],
            out_specs=vmem,
            scratch_shapes=[
                like(latent_in), like(shift_weight), like(scale_weight), like(gate_weight),
                like(down_query), like(down_latent), like(down_rope), like(up_query), like(up_key),
                like(up_value), like(out_weight), like(context_rope),
                pltpu.VMEM((rows, width), F32),
                pltpu.VMEM((group, 128), F32), pltpu.VMEM((group, 128), F32),
                pltpu.VMEM((group, 128), F32),
                pltpu.VMEM((sp, 4, shift_weight.shape[1]), F32),
                pltpu.VMEM((tp, 4, shift_weight.shape[1]), F32),
                pltpu.VMEM((sp, context_latent.shape[0], block), BF16),
                pltpu.VMEM((tp, sp, rows, block), BF16),
                pltpu.VMEM((tp, rows, q_rank), BF16),
                pltpu.VMEM((tp, rows, heads * V_HEAD), BF16),
                pltpu.VMEM((tp, rows, heads * V_HEAD), BF16),
                pltpu.VMEM((rows, width), F32),
                dma((13,)),
                dma((sp,)), dma((sp,)), dma((tp,)), dma((tp,)), dma((sp,)), dma((sp,)),
                dma((sp,)), dma((sp, tp)), dma((tp, sp)),
                dma((tp,)), dma((tp,)), dma((tp,)), dma((tp,)),
            ],
            compiler_params=pltpu.CompilerParams(
                collective_id=0, has_side_effects=True, vmem_limit_bytes=60 * 1024 * 1024
            ),
        )(
            latent_in, condition[None], context_latent, context_rope, shift_weight, scale_weight,
            gate_weight, norm_gain[None], down_query, down_latent, down_rope, query_gain[None],
            latent_gain[None], up_query, up_key, up_value, context_bias, out_weight, inverse,
        )

    in_specs = (
        P(("dp", "sp", "tp"), None), P(("dp", "sp")), P(("dp", "sp"), None), P(("dp", "sp"), None),
        P("sp", "tp"), P("sp", "tp"), P("sp", "tp"), P(), P(), P(), P(), P(), P(),
        P(None, "tp"), P(None, "tp"), P(None, "tp"), P("tp"), P(),
    )
    return jax.shard_map(
        on_device, mesh=mesh, in_specs=in_specs, out_specs=P(("dp", "sp", "tp"), None), check_vma=False
    )
```

time: 159 us -> 48.9 us (0.31)
  blocking collectives: 129 us -> 0 us
  Pallas kernels: 0 us -> 41.5 us
  matrix products: 18.4 us -> 0 us
  other arithmetic: 7.9 us -> 0.01 us
  local copies, waits for them, and re-layouts: 3.43 us -> 7.08 us
    all_gather x9 -> x0, blocking collectives: 107 us -> none  [the longest x1 16.9 us: on_device(): lax.all_gather(own_nope, 'sp', axis=0, tiled=True)]
    pallas_call x0 -> x1, Pallas kernels: none -> 41.5 us  [on_device(): pl.pallas_call(functools.partial(kernel, sp, tp), out_shape=jax.ShapeDtyp...]
    dot_general x18 -> x0, matrix products: 18.4 us -> none  [the longest x1 3.78 us: on_device(): mixed = jnp.dot(token_major, out_weight, preferred_element_type=jnp.float32)]
    psum x1 -> x0, blocking collectives: 13.8 us -> none  [on_device(): summed = lax.psum(partials, 'sp')]
    all_to_all x1 -> x0, blocking collectives: 8.09 us -> none  [on_device(): lax.all_to_all(attended, 'tp', split_axis=0, concat_axis=1, tiled=True)]
    unnamed x47 -> x3, local copies, waits for them, and re-layouts: 2.39 us -> 5.15 us
    reduce_sum x3 -> x0, other arithmetic: 2.49 us -> none  [the longest x2 1.28 us: attend(): new_total = run_total * shrink + jnp.sum(weights, axis=-1)]
where the time goes in v1:
time: 48.9 us; the launch traced here: 48.6 us
  Pallas kernels  41.5 us (85%)
  local copies, waits for them, and re-layouts  7.08 us (14%)
    pallas_call x1, Pallas kernels, on_device(): pl.pallas_call(functools.partial(kernel, sp, tp), out_shape=jax.ShapeDtyp...  41.5 us
    unnamed x3, local copies, waits for them, and re-layouts  5.15 us
    broadcast_in_dim x1, local copies, waits for them, and re-layouts, on_device(): condition[None]  1.27 us

profile of v1, /device:TPU:0, one launch (start us, length us, event | category | flops | bytes accessed | tf_op | source)
XLA Modules:
  0.0 48.6 jit_solution(6505390975533284657)
XLA Ops:
  0.0 1.3 %broadcast_in_dim.12.refs_1_ = bf16[1,512]{1,0:T(2,128)(2,1)} reshape(bf16[512]{0:T(512)(128)(2,1)} %param.19) | data formatting | bytes 2048 | tf_op jit(solution)/shard_map/broadcast_in_dim | solution.py:340
  1.3 0.7 %broadcast_in_dim_tile.3.refs_18_ = f32[1,128]{1,0:T(1,128)} reshape(f32[8,16]{1,0:T(8,128)S(1)} %tile.2) | data formatting | bytes 1024 | tf_op jit(solution)/shard_map/broadcast_in_dim;tile | solution.py:297
  1.9 1.4 %copy.19.refs_3_ = bf16[128,64]{1,0:T(8,128)(2,1)} copy(bf16[128,64]{0,1:T(8,128)(2,1)} %param.21) | data formatting | bytes 32768 | tf_op args[3]
  3.4 1.9 %copy.20.refs_10_ = bf16[2048,64]{1,0:T(8,128)(2,1)} copy(bf16[2048,64]{0,1:T(8,128)(2,1)} %param.28) | data formatting | bytes 524288 | tf_op args[10]
  5.3 41.5 %shard_map.172 = bf16[96,2048]{1,0:T(8,128)(2,1)} custom-call(bf16[96,2048]{1,0:T(8,128)(2,1)} %refs_0_.1, bf16[1,512]{1,0:T(2,128)(2,1)} %broadcast_in_dim.12.refs_1_, bf16[128,256]{1,0:T(8,128)(2,1)} %refs_2_.1, bf16[128,64]{1,0:T(8,128)(2,1)} %copy.19.refs_3_, bf16[512,512]{1,0:T(8,128)(2,1)} %refs_4_.1, bf16[512,512]{1,0:T(8,128)(2,1)} %refs_5_.1, ...), custom_call_target="tpu_custom_call" | custom-call | tf_op jit(solution)/shard_map/pallas_call | solution.py:310
  46.9 1.8 %copy.22 = bf16[96,2048]{1,0:T(8,128)(2,1)} copy(bf16[96,2048]{1,0:T(8,128)(2,1)} %shard_map.172) | data formatting | bytes 786432
  (2 shorter events, 0.0 us)

commit v2 on v1

--- a/solution.py
+++ b/solution.py
@@ -3,6 +3,7 @@
 
 import jax
 import jax.numpy as jnp
+import numpy as np
 from jax import lax
 from jax.experimental import pallas as pl
 from jax.experimental.pallas import tpu as pltpu
@@ -46,7 +47,7 @@
         x_ref, shift_w, scale_w, gate_w, dq, dl, dr, uq, uk, uv, ow, ctx_rope,
         base, cos_tab, sup_tab, sdn_tab, mod_z, mod_t, ctx_buf, lat_buf, q_buf, att_src, att_buf,
         mix, load_sem,
-        mz_send, mz_recv, mt_send, mt_recv, cx_send, cx_recv, lz_send, lt_send, l_recv,
+        mz_send, mz_recv, mt_send, mt_recv, cx_send, cx_recv, lz_send, lz_recv, lt_send, l_recv,
         q_send, q_recv, a_send, a_recv,
     ) = refs
     me_s = lax.axis_index("sp")
@@ -76,6 +77,7 @@
         ("uk", uk_hbm, uk), ("uv", uv_hbm, uv), ("uq", uq_hbm, uq), ("ow", ow_hbm, ow),
     )):
         loads[name] = pltpu.make_async_copy(src, dst, load_sem.at[i])
+    for name in ("shift", "scale", "gate", "cl", "cr", "x"):
         loads[name].start()
 
     barrier = pltpu.get_barrier_semaphore()
@@ -93,6 +95,8 @@
         loads[name].wait()
         mod_z[me_s, i:i + 1, :] = dot(act, w[...])[0:1]
     mod_z[me_s, 3:4, :] = jnp.zeros((1, mcol), F32)
+    for name in ("dl", "dr", "dq", "uk", "uv", "uq", "ow"):
+        loads[name].start()
     pl.semaphore_wait(barrier, sp + tp - 2)
     for d in range(1, sp):
         c = remote(mod_z.at[me_s], mod_z.at[me_s], mz_send.at[d], mz_recv.at[me_s], "sp", zpeer(d))
@@ -100,8 +104,9 @@
         sends.append(c)
     loads["cl"].wait()
     loads["cr"].wait()
-    cr = ctx_rope[...]
-    ctx_buf[me_s, :, kv_rank:] = jnp.concatenate([cr, cr], axis=1)
+    cr = ctx_rope[...].astype(F32)
+    cr = jnp.concatenate([cr, cr], axis=0)
+    ctx_buf[me_s, :, kv_rank:] = jnp.transpose(cr).astype(BF16)
     for d in range(1, sp):
         c = remote(ctx_buf.at[me_s], ctx_buf.at[me_s], cx_send.at[d], cx_recv.at[me_s], "sp", zpeer(d))
         c.start()
@@ -143,65 +148,98 @@
         m = mod_t[t]
         nd = (base[:, cols] * (1.0 + m[1:2]) + m[0:1]).astype(BF16)
         normed.append((nd, cols))
-        pl_, pr_ = dot(nd, dl[cols, :]), dot(nd, dr[cols, :])
+        pl_, pr_ = dot(nd, dl[cols, :]), dot_t(nd, dr[:, cols])
         low_l = pl_ if low_l is None else low_l + pl_
         low_r = pr_ if low_r is None else low_r + pr_
     own = pl.ds(pl.multiple_of(me_t * rows, rows), rows)
-    lat_buf[me_t, me_s, :, :kv_rank] = rms(low_l, l_gain_ref[...]).astype(BF16)
-    lat_buf[me_t, me_s, :, kv_rank:] = turn(
+    lat_buf[me_t, me_s, :rows, :] = rms(low_l, l_gain_ref[...]).astype(BF16)
+    rk = turn(
         jnp.concatenate([low_r, low_r], axis=1), cos_tab[own, :], sup_tab[own, :], sdn_tab[own, :]
-    ).astype(BF16)
+    )
+    fold = lat_buf.shape[2] - rows
+    fold_low = lax.broadcasted_iota(jnp.int32, (fold, 128), 1) < 64
+    packed = [
+        jnp.where(fold_low, rk[2 * j * fold:(2 * j + 1) * fold], rk[(2 * j + 1) * fold:(2 * j + 2) * fold])
+        for j in range(rows // fold // 2)
+    ]
+    lat_buf[me_t, me_s, rows:, :] = jnp.concatenate(packed, axis=1).astype(BF16)
     mine = lat_buf.at[me_t, me_s]
-    for d in range(1, sp):
-        c = remote(mine, mine, lz_send.at[d], l_recv.at[me_t, me_s], "sp", zpeer(d))
-        c.start()
-        sends.append(c)
+
+    near = (lax.bitwise_xor(me_t, 1), lax.bitwise_xor(me_t, 2))
+    far = lax.bitwise_xor(me_t, 3)
+
+    def half(ref, k):
+        cut = ref.shape[0] // 32 * 16
+        return ref.at[pl.ds(0, cut)] if k == 0 else ref.at[pl.ds(cut, ref.shape[0] - cut)]
+
+    def share(view, ssem, rsem, at):
+        for k in range(2):
+            c = remote(view, view, ssem.at[(*at, k)], rsem.at[(me_t, *at, 0)], "tp", near[k])
+            c.start()
+            sends.append(c)
+
+    def relay(view, ssem, rsem, at, k):
+        remote(view, view, ssem.at[(*at, k)], rsem.at[(near[k], *at, 0)], "tp", near[k]).wait_recv()
+        piece = half(view, k)
+        c = remote(piece, piece, ssem.at[(*at, 2 + k)], rsem.at[(near[k], *at, k)], "tp", near[1 - k])
+        c.start()
+        sends.append(c)
+
+    def finish(view, ssem, rsem, at):
+        for k in range(2):
+            piece = half(view, k)
+            remote(piece, piece, ssem.at[(*at, 2 + k)], rsem.at[(far, *at, k)], "tp", near[1 - k]).wait_recv()
+
+    for d in range(1, sp):
+        c = remote(mine, mine, lz_send.at[d], lz_recv.at[me_s], "sp", zpeer(d))
+        c.start()
+        sends.append(c)
+    share(mine, lt_send, l_recv, (me_s,))
     loads["dq"].wait()
     low_q = None
     for nd, cols in normed:
         pq = dot(nd, dq[cols, :])
         low_q = pq if low_q is None else low_q + pq
     q_buf[me_t] = rms(low_q, q_gain_ref[...]).astype(BF16)
-    for d in range(1, tp):
-        c = remote(q_buf.at[me_t], q_buf.at[me_t], q_send.at[d], q_recv.at[me_t], "tp", tpeer(d))
-        c.start()
-        sends.append(c)
-    for d in range(1, tp):
-        c = remote(mine, mine, lt_send.at[0, d], l_recv.at[me_t, me_s], "tp", tpeer(d))
-        c.start()
-        sends.append(c)
-
-    def expand(block):
-        low = block[:, :kv_rank]
+    share(q_buf.at[me_t], q_send, q_recv, ())
+
+    def unfold(part):
+        turned = []
+        for j in range(part.shape[1] // 128):
+            a = part[:, 128 * j:128 * (j + 1)].astype(F32)
+            b = pltpu.roll(a, 64, 1)
+            turned += [jnp.where(fold_low, a, b), jnp.where(fold_low, b, a)]
+        return jnp.concatenate(turned, axis=0).astype(BF16)
+
+    def expand(low, kr):
         kn = dot(low, uk[...]).astype(BF16)
         v = dot(low, uv[...]).astype(BF16)
-        kr = block[:, kv_rank:]
         return (
             jnp.concatenate([kn[:, :QK_NOPE], kr], axis=1),
             jnp.concatenate([kn[:, QK_NOPE:], kr], axis=1),
             v,
         )
 
+    for k in range(2):
+        relay(lat_buf.at[near[k], me_s], lt_send, l_recv, (me_s,), k)
+    for k in range(2):
+        relay(q_buf.at[near[k]], q_send, q_recv, (), k)
+    for d in range(1, sp):
+        s = zpeer(d)
+        slot = lat_buf.at[me_t, s]
+        remote(slot, slot, lz_send.at[d], lz_recv.at[s], "sp", s).wait_recv()
+        share(slot, lt_send, l_recv, (s,))
+
     loads["uk"].wait()
     loads["uv"].wait()
     for d in range(1, sp):
         s = zpeer(d)
         remote(ctx_buf.at[s], ctx_buf.at[s], cx_send.at[d], cx_recv.at[s], "sp", s).wait_recv()
-    ctx_kv = expand(ctx_buf[...].reshape(-1, ctx_buf.shape[2]))
-
-    for d in range(1, sp):
-        s = zpeer(d)
-        slot = lat_buf.at[me_t, s]
-        remote(slot, slot, lz_send.at[d], l_recv.at[me_t, s], "sp", s).wait_recv()
-        for e in range(1, tp):
-            c = remote(slot, slot, lt_send.at[d, e], l_recv.at[me_t, s], "tp", tpeer(e))
-            c.start()
-            sends.append(c)
+    ctx_all = ctx_buf[...].reshape(-1, ctx_buf.shape[2])
+    ctx_kv = expand(ctx_all[:, :kv_rank], ctx_all[:, kv_rank:])
 
     loads["uq"].wait()
-    for d in range(1, tp):
-        t = tpeer(d)
-        remote(q_buf.at[t], q_buf.at[t], q_send.at[d], q_recv.at[t], "tp", t).wait_recv()
+    finish(q_buf.at[far], q_send, q_recv, ())
     q = dot(q_buf[...].reshape(group, q_buf.shape[2]), uq[...])
     one, two = q[:, 128:256], q[:, 256:384]
     low_half = lax.broadcasted_iota(jnp.int32, (group, 128), 1) < 64
@@ -238,17 +276,22 @@
 
     state = attend(None, ctx_kv, True)
     span = math.gcd(sp, 4)
-    for d in range(tp):
-        t = tpeer(d)
-        if d:
+    for d, t in enumerate((me_t, *near, far)):
+        if d == 1:
+            for e in range(1, sp):
+                s = zpeer(e)
+                for k in range(2):
+                    relay(lat_buf.at[near[k], s], lt_send, l_recv, (s,), k)
+        if d == 3:
             for e in range(sp):
                 s = zpeer(e)
-                slot = lat_buf.at[t, s]
-                remote(slot, slot, lt_send.at[e, d], l_recv.at[t, s], "tp", t).wait_recv()
+                finish(lat_buf.at[far, s], lt_send, l_recv, (s,))
 
         def chunk(i, st, t=t):
             block = lat_buf[t, pl.ds(i * span, span)]
-            return attend(st, expand(block.reshape(span * rows, block.shape[2])), False)
+            low = jnp.concatenate([block[j, :rows] for j in range(span)], axis=0)
+            kr = jnp.concatenate([unfold(block[j, rows:]) for j in range(span)], axis=0)
+            return attend(st, expand(low, kr), False)
 
         if sp == span:
             state = chunk(0, state)
@@ -293,8 +336,8 @@
     ):
         rows, width = latent_in.shape
         n = QK_ROPE // 4
-        inverse = ROPE_BASE ** (-jnp.arange(n, dtype=F32) / n)
-        inverse = jnp.tile(inverse, 128 // n)[None]
+        inverse = np.tile(np.float32(ROPE_BASE) ** (-np.arange(n, dtype=np.float32) / n), 128 // n)
+        inverse = inverse.astype(np.float32)[None]
         group = rows * tp
         any_ = pl.BlockSpec(memory_space=pl.ANY)
         vmem = pl.BlockSpec(memory_space=pltpu.VMEM)
@@ -315,30 +358,30 @@
             out_specs=vmem,
             scratch_shapes=[
                 like(latent_in), like(shift_weight), like(scale_weight), like(gate_weight),
-                like(down_query), like(down_latent), like(down_rope), like(up_query), like(up_key),
-                like(up_value), like(out_weight), like(context_rope),
+                like(down_query), like(down_latent), like(down_rope.T), like(up_query), like(up_key),
+                like(up_value), like(out_weight), like(context_rope.T),
                 pltpu.VMEM((rows, width), F32),
                 pltpu.VMEM((group, 128), F32), pltpu.VMEM((group, 128), F32),
                 pltpu.VMEM((group, 128), F32),
                 pltpu.VMEM((sp, 4, shift_weight.shape[1]), F32),
                 pltpu.VMEM((tp, 4, shift_weight.shape[1]), F32),
                 pltpu.VMEM((sp, context_latent.shape[0], block), BF16),
-                pltpu.VMEM((tp, sp, rows, block), BF16),
+                pltpu.VMEM((tp, sp, rows + rows * QK_ROPE // kv_rank, kv_rank), BF16),
                 pltpu.VMEM((tp, rows, q_rank), BF16),
                 pltpu.VMEM((tp, rows, heads * V_HEAD), BF16),
                 pltpu.VMEM((tp, rows, heads * V_HEAD), BF16),
                 pltpu.VMEM((rows, width), F32),
                 dma((13,)),
                 dma((sp,)), dma((sp,)), dma((tp,)), dma((tp,)), dma((sp,)), dma((sp,)),
-                dma((sp,)), dma((sp, tp)), dma((tp, sp)),
-                dma((tp,)), dma((tp,)), dma((tp,)), dma((tp,)),
+                dma((sp,)), dma((sp,)), dma((sp, 4)), dma((tp, sp, 2)),
+                dma((4,)), dma((tp, 2)), dma((tp,)), dma((tp,)),
             ],
             compiler_params=pltpu.CompilerParams(
                 collective_id=0, has_side_effects=True, vmem_limit_bytes=60 * 1024 * 1024
             ),
         )(
-            latent_in, condition[None], context_latent, context_rope, shift_weight, scale_weight,
-            gate_weight, norm_gain[None], down_query, down_latent, down_rope, query_gain[None],
+            latent_in, condition[None], context_latent, context_rope.T, shift_weight, scale_weight,
+            gate_weight, norm_gain[None], down_query, down_latent, down_rope.T, query_gain[None],
             latent_gain[None], up_query, up_key, up_value, context_bias, out_weight, inverse,
         )
 

time: 48.9 us -> 41 us (0.84)
  local copies, waits for them, and re-layouts: 7.08 us -> 3.03 us
  Pallas kernels: 41.5 us -> 37.7 us
    pallas_call x1, Pallas kernels: 41.5 us -> 37.7 us  [on_device(): pl.pallas_call(functools.partial(kernel, sp, tp), out_shape=jax.ShapeDtyp...]
    unnamed x3 -> x1, local copies, waits for them, and re-layouts: 5.15 us -> 1.77 us
    another operation x2 -> x0, local copies, waits for them, and re-layouts: 0.66 us -> none  [on_device(): inverse = jnp.tile(inverse, 128 // n)[None]]
where the time goes in v2:
time: 41 us; the launch traced here: 40.8 us
  Pallas kernels  37.7 us (92%)
  local copies, waits for them, and re-layouts  3.03 us (7%)
    pallas_call x1, Pallas kernels, on_device(): pl.pallas_call(functools.partial(kernel, sp, tp), out_shape=jax.ShapeDtyp...  37.7 us
    unnamed x1, local copies, waits for them, and re-layouts  1.77 us
    broadcast_in_dim x1, local copies, waits for them, and re-layouts, on_device(): condition[None]  1.26 us

profile of v2, /device:TPU:0, one launch (start us, length us, event | category | flops | bytes accessed | tf_op | source)
XLA Modules:
  0.0 40.8 jit_solution(464418611713222962)
XLA Ops:
  0.0 1.3 %broadcast_in_dim.12.refs_1_ = bf16[1,512]{1,0:T(2,128)(2,1)} reshape(bf16[512]{0:T(512)(128)(2,1)} %param.20) | data formatting | bytes 2048 | tf_op jit(solution)/shard_map/broadcast_in_dim | solution.py:383
  1.3 37.7 %shard_map.181 = bf16[96,2048]{1,0:T(8,128)(2,1)} custom-call(bf16[96,2048]{1,0:T(8,128)(2,1)} %refs_0_.1, bf16[1,512]{1,0:T(2,128)(2,1)} %broadcast_in_dim.12.refs_1_, bf16[128,256]{1,0:T(8,128)(2,1)} %refs_2_.1, bf16[64,128]{1,0:T(8,128)(2,1)} %bitcast.6, bf16[512,512]{1,0:T(8,128)(2,1)} %refs_4_.1, bf16[512,512]{1,0:T(8,128)(2,1)} %refs_5_.1, ...), custom_call_target="tpu_custom_call" | custom-call | tf_op jit(solution)/shard_map/pallas_call | solution.py:353
  39.0 1.8 %copy.21 = bf16[96,2048]{1,0:T(8,128)(2,1)} copy(bf16[96,2048]{1,0:T(8,128)(2,1)} %shard_map.181) | data formatting | bytes 786432
